TPU v7x, 512 devices: a whole 4x4x16 slice. The times are simulated.
512 devices in a mesh: ep: 16 (over y, x), tp: 32 (over z, core).
Axes of the slice: x: 4, y: 4, z: 16, core: 2. Of those that a mesh axis runs over, the one named last changes fastest.
Arguments:
- features: bfloat16 [256, 1024], P('ep', 'tp'), may hold values from -6 to 6
- key_table: bfloat16 [262144, 1024], P('ep', 'tp'), may hold values from -0.1875 to 0.1875
- value_table: bfloat16 [262144, 1024], P('ep', 'tp'), may hold values from -6 to 6
- chosen: int32 [256, 4, 16], P('ep'), may hold values from 0 to 262143
- scores: float32 [256, 4, 16], P('ep'), may hold values from -8 to 8
Outputs:
- mixed: bfloat16 [256, 1024], P('ep', 'tp')
Inputs may be any that keep to these rules, and one draw needn't show every extreme that they name: Every chosen row is a row of the tables, 0 to 262143; rows may repeat, and a few rows are far more popular than the rest.
All inputs are finite; a program needn't handle non-finite values.
Results may differ from a plain program's by a relative error of at most 0.0065.
Values may be sent and summed in bfloat16 or wider, within the bound.
A program may use at most 64 MiB of HBM per device.

v0:
```python
import jax
import jax.numpy as jnp
from jax import lax
from jax.sharding import Mesh
from jax.sharding import PartitionSpec as P

EP = ("ep_0", "ep_1")


def gathered_by_axis(shard, axes, dim):
    if not axes:
        return shard
    nearer = lax.all_gather(shard, axes[-1], axis=dim, tiled=True)
    return gathered_by_axis(nearer, axes[:-1], dim)


def over_pieces(shard, axis):
    return lax.all_gather(shard, axis).sum(0)


def cut_along(shard, dim, peers):
    dims = shard.shape
    blocks = shard.reshape(*dims[:dim], peers, dims[dim] // peers, *dims[dim + 1 :])
    return jnp.moveaxis(blocks, dim, 0)


def cut_rows(length, count):
    step = length // count
    if step >= 8:
        step -= step % 8
    return [step * k for k in range(1, count)]


def reduced_to_own(blocks, axes, order):
    dims = [lax.axis_size(a) for a in axes]
    blocks = blocks.reshape(*dims, *blocks.shape[1:])
    blocks = blocks.transpose(*order, *range(len(axes), blocks.ndim))
    blocks = blocks.reshape(-1, *blocks.shape[len(axes) :])
    for k in order:
        blocks = lax.psum_scatter(blocks, axes[k], scatter_dimension=0, tiled=True)
    return blocks[0]


def spread_scatter(shard, axes, dim):
    blocks = cut_along(shard, dim, lax.axis_size(axes))
    cut = max(range(1, max(2, blocks.ndim - 1)), key=lambda d: blocks.shape[d])
    count, done = len(axes), []
    for initial, slab in enumerate(jnp.split(blocks, cut_rows(blocks.shape[cut], count), axis=cut)):
        if slab.size:
            order = [(initial + k) % count for k in range(count)]
            done.append(reduced_to_own(slab, axes, order))
    return jnp.concatenate(done, axis=cut - 1)


def in_blocks(func, arrays):
    total = arrays[0].shape[0]
    width = 32 if total % 32 == 0 else total
    count = total // width
    if count == 1:
        return func(arrays)
    shaped = tuple((item.reshape((count, width) + item.shape[1:]) for item in arrays))
    result = lax.map(func, shaped)
    return result.reshape((total,) + result.shape[2:])


def local(features, key_table, value_table, chosen, scores):
    table_rows = key_table.shape[0]
    head_count = chosen.shape[1]
    top_count = chosen.shape[2]
    first_row = lax.axis_index(EP) * table_rows
    gate_weights = jax.nn.softmax(scores, axis=-1)
    chosen_all = gathered_by_axis(chosen, EP, 0)
    gates_all = lax.all_gather(gate_weights, EP, axis=0, tiled=True)
    shifted = chosen_all - first_row
    owned_mask = (shifted >= 0) & (shifted < table_rows)
    local_rows = jnp.clip(shifted, 0, table_rows - 1).reshape(shifted.shape[0], -1)

    def dots_block(pair):
        token_block, picked = pair
        dense = lax.dot_general(
            token_block, key_table, (((1,), (1,)), ((), ())), preferred_element_type=jnp.float32
        )
        return jnp.take_along_axis(dense, picked, axis=1)

    def partial_dots(token_block):
        row_count = token_block.shape[0]
        picked = lax.slice_in_dim(local_rows, 0, row_count, axis=0)
        keep_mask = lax.slice_in_dim(owned_mask, 0, row_count, axis=0)
        products = in_blocks(dots_block, (token_block, picked))
        return jnp.where(keep_mask.reshape(row_count, -1), products, 0.0)

    partial_value = partial_dots(lax.all_gather(features, EP, axis=0, tiled=True))
    partial_value = partial_value.reshape(-1, head_count, top_count)
    products = over_pieces(partial_value, "tp")
    row_weights = (gates_all * jax.nn.gelu(products, approximate=False)).astype(jnp.bfloat16)
    row_weights = jnp.where(owned_mask, row_weights, jnp.zeros_like(row_weights))
    flat_weights = row_weights.reshape(row_weights.shape[0], -1)

    def value_block(pair):
        block_weights, picked = pair
        width = picked.shape[0]
        token_ids = lax.broadcasted_iota(jnp.int32, picked.shape, 0)
        dense = (
            jnp.zeros((width, table_rows), jnp.float32)
            .at[token_ids, picked]
            .add(block_weights.astype(jnp.float32))
        )
        upper = dense.astype(jnp.bfloat16)
        lower = (dense - upper.astype(jnp.float32)).astype(jnp.bfloat16)
        summed = jnp.dot(upper, value_table, preferred_element_type=jnp.float32)
        return summed + jnp.dot(lower, value_table, preferred_element_type=jnp.float32)

    def owner_term(row_count):
        picked = lax.slice_in_dim(local_rows, 0, row_count, axis=0)
        block_weights = lax.slice_in_dim(flat_weights, 0, row_count, axis=0)
        return in_blocks(value_block, (block_weights, picked))

    summed = spread_scatter(owner_term(features.shape[0] * lax.axis_size(EP)), EP, 0)
    return summed.astype(jnp.bfloat16)


def solution(mesh):
    torus = Mesh(mesh.devices.reshape(4, 4, mesh.shape["tp"]), ("ep_0", "ep_1", "tp"))
    in_specs = (P(EP, "tp"), P(EP, "tp"), P(EP, "tp"), P(EP, None, None), P(EP, None, None))
    out_specs = P(EP, "tp")
    return jax.shard_map(local, mesh=torus, in_specs=in_specs, out_specs=out_specs, check_vma=False)
```

profile of v0, /device:TPU:1, one launch (start us, length us, event | category | flops | bytes accessed | tf_op | source)
XLA Modules:
  0.0 512.8 jit_solution(13404930220710926609)
XLA Ops:
  6.5 10.6 %all_gather.15 = s32[64,4,16]{2,1,0:T(4,128)S(1)} all-gather(s32[16,4,16]{2,1,0:T(4,128)} %param.12), channel_id=1, replica_groups=mesh['ep_0'=4,'ep_1'=4,'tp'=32] {'ep_1'}, dimensions={0}, use_global_device_ids=true | all-gather | bytes 20480 | tf_op jit(solution)/shard_map/all_gather | solution.py:13
  17.2 10.4 %all_gather.16 = s32[256,4,16]{2,1,0:T(4,128)S(1)} all-gather(s32[64,4,16]{2,1,0:T(4,128)S(1)} %all_gather.15), channel_id=1, replica_groups=mesh['ep_0'=4,'ep_1'=4,'tp'=32] {'ep_0'}, dimensions={0}, use_global_device_ids=true | all-gather | bytes 81920 | tf_op jit(solution)/shard_map/all_gather | solution.py:13
  28.0 18.3 %all_gather.18 = bf16[256,32]{1,0:T(8,128)(2,1)S(1)} all-gather(bf16[16,32]{1,0:T(8,128)(2,1)S(1)} %copy-done.2), channel_id=1, replica_groups=mesh['ep_0'=4,'ep_1'=4,'tp'=32] {'ep_0','ep_1'}, dimensions={0}, use_global_device_ids=true | all-gather | bytes 17408 | tf_op jit(solution)/shard_map/all_gather | solution.py:92
  46.4 142.8 %while.20 = (s32[]{:T(128)}, f32[8,32,64]{2,1,0:T(8,128)}, s32[8,32,64]{2,1,0:T(8,128)S(1)}, bf16[8,32,32]{2,1,0:T(8,128)(2,1)S(1)}, bf16[16384,32]{0,1:T(8,128)(2,1)S(1)}, /*index=5*/s32[]{:T(128)}) while((s32[]{:T(128)}, f32[8,32,64]{2,1,0:T(8,128)}, s32[8,32,64]{2,1,0:T(8,128)S(1)}, bf16[8,32,32]{2,1,0:T(8,128)(2,1)S(1)}, ...), condition=%wide.region_3.4_spmd, body=%wide.region_2.3_spmd.sunk | while | flops 33585152 | bytes 3269197 | solution.py:62
  46.9 16.6 %gather_fusion = f32[2048]{0:T(1024)S(1)} fusion(f32[32,16384]{1,0:T(8,128)S(1)} %fusion.50, s32[2048]{0:T(1024)S(1)} %reshape.136), kind=kCustom, calls=%fused_computation.clone.1 | custom fusion | bytes 32768 | tf_op jit(solution)/shard_map/while/body/eval_jaxpr/jit(take_along_axis)/gather | solution.py:83
  64.8 16.6 %gather_fusion = f32[2048]{0:T(1024)S(1)} fusion(f32[32,16384]{1,0:T(8,128)S(1)} %fusion.50, s32[2048]{0:T(1024)S(1)} %reshape.136), kind=kCustom, calls=%fused_computation.clone.1 | custom fusion | bytes 32768 | tf_op jit(solution)/shard_map/while/body/eval_jaxpr/jit(take_along_axis)/gather | solution.py:83
  82.6 16.6 %gather_fusion = f32[2048]{0:T(1024)S(1)} fusion(f32[32,16384]{1,0:T(8,128)S(1)} %fusion.50, s32[2048]{0:T(1024)S(1)} %reshape.136), kind=kCustom, calls=%fused_computation.clone.1 | custom fusion | bytes 32768 | tf_op jit(solution)/shard_map/while/body/eval_jaxpr/jit(take_along_axis)/gather | solution.py:83
  100.4 16.6 %gather_fusion = f32[2048]{0:T(1024)S(1)} fusion(f32[32,16384]{1,0:T(8,128)S(1)} %fusion.50, s32[2048]{0:T(1024)S(1)} %reshape.136), kind=kCustom, calls=%fused_computation.clone.1 | custom fusion | bytes 32768 | tf_op jit(solution)/shard_map/while/body/eval_jaxpr/jit(take_along_axis)/gather | solution.py:83
  118.3 16.6 %gather_fusion = f32[2048]{0:T(1024)S(1)} fusion(f32[32,16384]{1,0:T(8,128)S(1)} %fusion.50, s32[2048]{0:T(1024)S(1)} %reshape.136), kind=kCustom, calls=%fused_computation.clone.1 | custom fusion | bytes 32768 | tf_op jit(solution)/shard_map/while/body/eval_jaxpr/jit(take_along_axis)/gather | solution.py:83
  136.1 16.6 %gather_fusion = f32[2048]{0:T(1024)S(1)} fusion(f32[32,16384]{1,0:T(8,128)S(1)} %fusion.50, s32[2048]{0:T(1024)S(1)} %reshape.136), kind=kCustom, calls=%fused_computation.clone.1 | custom fusion | bytes 32768 | tf_op jit(solution)/shard_map/while/body/eval_jaxpr/jit(take_along_axis)/gather | solution.py:83
  154.0 16.6 %gather_fusion = f32[2048]{0:T(1024)S(1)} fusion(f32[32,16384]{1,0:T(8,128)S(1)} %fusion.50, s32[2048]{0:T(1024)S(1)} %reshape.136), kind=kCustom, calls=%fused_computation.clone.1 | custom fusion | bytes 32768 | tf_op jit(solution)/shard_map/while/body/eval_jaxpr/jit(take_along_axis)/gather | solution.py:83
  171.8 16.6 %gather_fusion = f32[2048]{0:T(1024)S(1)} fusion(f32[32,16384]{1,0:T(8,128)S(1)} %fusion.50, s32[2048]{0:T(1024)S(1)} %reshape.136), kind=kCustom, calls=%fused_computation.clone.1 | custom fusion | bytes 32768 | tf_op jit(solution)/shard_map/while/body/eval_jaxpr/jit(take_along_axis)/gather | solution.py:83
  191.3 17.3 %all_gather.17 = f32[256,4,16]{2,1,0:T(4,128)S(1)} all-gather(f32[16,4,16]{2,1,0:T(4,128)S(1)} %fusion.17), channel_id=1, replica_groups=mesh['ep_0'=4,'ep_1'=4,'tp'=32] {'ep_0','ep_1'}, dimensions={0}, use_global_device_ids=true | all-gather | bytes 69632 | tf_op jit(solution)/shard_map/all_gather | solution.py:73
  208.7 66.9 %all-gather.3.cloned.1.call-done = f32[8192,4,16]{0,2,1:T(8,128)} async-done(((f32[256,4,16]{0,2,1:T(8,128)}), f32[8192,4,16]{0,2,1:T(8,128)}) %all-gather.3.cloned.1.call-update) | async-done | bytes 2097168 | tf_op jit(solution)/shard_map/all_gather | solution.py:18
  275.6 2.2 copy.21
  279.0 157.2 %while.21 = (s32[]{:T(128)}, f32[8,32,32]{2,1,0:T(8,128)S(1)}, s32[8,32,64]{2,1,0:T(8,128)S(1)}, bf16[8,32,64]{2,1,0:T(8,128)(2,1)S(1)}, bf16[16384,32]{0,1:T(8,...) while((s32[]{:T(128)}, f32[8,32,32]{2,1,0:T(8,128)S(1)}, s32[8,32,64]{2,1,0:T(8,128)S(1)}, ...), condition=%wide.region_7.8_spmd, body=%wide.region_5.7_spmd.sunk | while | flops 69772288 | bytes 12750973 | solution.py:62
  280.7 15.5 %scatter_custom_fusion.5 = f32[524288]{0:T(1024)} fusion(s32[2048]{0:T(1024)S(1)} %reshape.139, f32[2048]{0:T(1024)S(1)} %reshape.140, f32[]{:T(128)} %constant.62.clone.1..sunk), kind=kCustom, calls=%fused_computation.16.clone.1 | custom fusion | flops 2048 | bytes 2097156 | tf_op jit(solution)/shard_map/while
  296.1 1.7 reshape.141
  300.4 15.3 %scatter_custom_fusion.5 = f32[524288]{0:T(1024)} fusion(s32[2048]{0:T(1024)S(1)} %reshape.139, f32[2048]{0:T(1024)S(1)} %reshape.140, f32[]{:T(128)} %constant.62.clone.1..sunk), kind=kCustom, calls=%fused_computation.16.clone.1 | custom fusion | flops 2048 | bytes 2097156 | tf_op jit(solution)/shard_map/while
  315.7 1.7 reshape.141
  320.0 15.4 %scatter_custom_fusion.5 = f32[524288]{0:T(1024)} fusion(s32[2048]{0:T(1024)S(1)} %reshape.139, f32[2048]{0:T(1024)S(1)} %reshape.140, f32[]{:T(128)} %constant.62.clone.1..sunk), kind=kCustom, calls=%fused_computation.16.clone.1 | custom fusion | flops 2048 | bytes 2097156 | tf_op jit(solution)/shard_map/while
  335.3 1.7 reshape.141
  339.6 15.4 %scatter_custom_fusion.5 = f32[524288]{0:T(1024)} fusion(s32[2048]{0:T(1024)S(1)} %reshape.139, f32[2048]{0:T(1024)S(1)} %reshape.140, f32[]{:T(128)} %constant.62.clone.1..sunk), kind=kCustom, calls=%fused_computation.16.clone.1 | custom fusion | flops 2048 | bytes 2097156 | tf_op jit(solution)/shard_map/while
  355.0 1.7 reshape.141
  359.3 15.4 %scatter_custom_fusion.5 = f32[524288]{0:T(1024)} fusion(s32[2048]{0:T(1024)S(1)} %reshape.139, f32[2048]{0:T(1024)S(1)} %reshape.140, f32[]{:T(128)} %constant.62.clone.1..sunk), kind=kCustom, calls=%fused_computation.16.clone.1 | custom fusion | flops 2048 | bytes 2097156 | tf_op jit(solution)/shard_map/while
  379.0 15.4 %scatter_custom_fusion.5 = f32[524288]{0:T(1024)} fusion(s32[2048]{0:T(1024)S(1)} %reshape.139, f32[2048]{0:T(1024)S(1)} %reshape.140, f32[]{:T(128)} %constant.62.clone.1..sunk), kind=kCustom, calls=%fused_computation.16.clone.1 | custom fusion | flops 2048 | bytes 2097156 | tf_op jit(solution)/shard_map/while
  398.6 15.3 %scatter_custom_fusion.5 = f32[524288]{0:T(1024)} fusion(s32[2048]{0:T(1024)S(1)} %reshape.139, f32[2048]{0:T(1024)S(1)} %reshape.140, f32[]{:T(128)} %constant.62.clone.1..sunk), kind=kCustom, calls=%fused_computation.16.clone.1 | custom fusion | flops 2048 | bytes 2097156 | tf_op jit(solution)/shard_map/while
  418.2 15.4 %scatter_custom_fusion.5 = f32[524288]{0:T(1024)} fusion(s32[2048]{0:T(1024)S(1)} %reshape.139, f32[2048]{0:T(1024)S(1)} %reshape.140, f32[]{:T(128)} %constant.62.clone.1..sunk), kind=kCustom, calls=%fused_computation.16.clone.1 | custom fusion | flops 2048 | bytes 2097156 | tf_op jit(solution)/shard_map/while
  440.2 20.2 %reduce-scatter.5.cloned.1.call-done = f32[4,8,32]{2,1,0:T(8,128)} async-done(((f32[16,8,32]{2,1,0:T(8,128)}), f32[4,8,32]{2,1,0:T(8,128)}) %reduce-scatter.5.cloned.1.call-update) | async-done | bytes 4112 | tf_op jit(solution)/shard_map/reduce_scatter | solution.py:40
  460.4 13.8 %all-reduce.1 = bf16[4,8,32]{2,1,0:T(8,128)(2,1)S(1)} all-reduce(f32[4,8,32]{2,1,0:T(8,128)} %reduce-scatter.5.cloned.1.call-done), channel_id=6, replica_groups=mesh['ep_0'=4,'ep_1'=4,'tp'=32] {'ep_0'}, use_global_device_ids=true, to_apply=%region_11.12.clone | all-reduce | flops 1024 | bytes 6144
  474.8 16.4 %reduce-scatter.3.cloned.1.call-done = f32[4,8,32]{2,1,0:T(8,128)} async-done(((f32[16,8,32]{2,1,0:T(8,128)}), f32[4,8,32]{2,1,0:T(8,128)}) %reduce-scatter.3.cloned.1.call-update) | async-done | bytes 4112 | tf_op jit(solution)/shard_map/reduce_scatter | solution.py:40
  491.2 13.7 %all-reduce = bf16[4,8,32]{2,1,0:T(8,128)(2,1)S(1)} all-reduce(f32[4,8,32]{2,1,0:T(8,128)} %reduce-scatter.3.cloned.1.call-done), channel_id=4, replica_groups=mesh['ep_0'=4,'ep_1'=4,'tp'=32] {'ep_1'}, use_global_device_ids=true, to_apply=%region_9.10.clone | all-reduce | flops 1024 | bytes 6144
  (160 shorter events, 46.0 us)
Async XLA Ops:
  6.5 21.5 %copy-start.2 = (bf16[16,32]{1,0:T(8,128)(2,1)S(1)}, bf16[16,32]{1,0:T(8,128)(2,1)}, u32[]{:S(2)}) copy-start(bf16[16,32]{1,0:T(8,128)(2,1)} %param.9) | copy-start | bytes 3076
  6.5 39.8 %copy-start.1 = (bf16[16384,32]{0,1:T(8,128)(2,1)S(1)}, bf16[16384,32]{0,1:T(8,128)(2,1)}, u32[]{:S(2)}) copy-start(bf16[16384,32]{0,1:T(8,128)(2,1)} %param.10) | copy-start | bytes 3145732
  6.5 269.0 %all-gather.3.cloned.1.call-start = ((), (), s32[]{:S(2)}) async-start(), calls=%async_computation.4 | async-start | bytes 2162688 | tf_op jit(solution)/shard_map/all_gather | solution.py:18
  46.3 144.7 %copy-start.3 = (f32[16,4,16]{2,1,0:T(4,128)S(1)}, f32[16,4,16]{2,1,0:T(4,128)}, u32[]{:S(2)}) copy-start(f32[16,4,16]{2,1,0:T(4,128)} %param.13) | copy-start | bytes 12292
  191.0 269.4 %reduce-scatter.5.cloned.1.call-start = ((), (), s32[]{:S(2)}) async-start(), calls=%async_computation.3 | async-start | bytes 81920 | tf_op jit(solution)/shard_map/reduce_scatter | solution.py:40
  277.8 1.2 copy-start
  437.5 53.7 %reduce-scatter.3.cloned.1.call-start = ((), (), s32[]{:S(2)}) async-start(), calls=%async_computation.2 | async-start | bytes 81920 | tf_op jit(solution)/shard_map/reduce_scatter | solution.py:40
Sparse Core Ops, SparseCore 0:
  191.1 84.4 all-gather.2
  437.6 22.7 reduce-scatter.4
  463.2 28.0 reduce-scatter.2
where the time goes:
time: 518 us; the launch traced here: 513 us
  local copies, waits for them, and re-layouts  159 us (31%)
  other arithmetic  142 us (27%)
  waiting for transfers between devices  104 us (20%)
  blocking collectives  84.1 us (16%)
  between operations  13.3 us (3%)
  matrix products  10.1 us (2%)
    while x32, other arithmetic  135 us
    gather x24, local copies, waits for them, and re-layouts, dots_block(): return jnp.take_along_axis(dense, picked, axis=1)  134 us
    all_gather x1, waiting for transfers between devices, over_pieces(): return lax.all_gather(shard, axis).sum(0)  66.9 us
    reduce_scatter x2, waiting for transfers between devices, reduced_to_own(): blocks = lax.psum_scatter(blocks, axes[k], scatter_dimension=0, tiled=True)  36.6 us
    unnamed x2, blocking collectives  27.5 us
    all_gather x2, blocking collectives, gathered_by_axis(): nearer = lax.all_gather(shard, axes[-1], axis=dim, tiled=True)  21 us
    all_gather x1, blocking collectives, local(): lax.all_gather(features, EP, axis=0, tiled=True)  18.3 us
    all_gather x1, blocking collectives, local(): gates_all = lax.all_gather(gate_weights, EP, axis=0, tiled=True)  17.3 us
  transfers between devices with their start and end apart: 3, of which 3 were waited for; matrix products, arithmetic and copies ran while one was open for 1% of the time, Pallas kernels for 0%

commit v1 on v0

v1 whole, which is shorter than its diff:
```python
import functools

import jax
import jax.numpy as jnp
from jax import lax
from jax.experimental import pallas as pl
from jax.experimental.pallas import tpu as pltpu
from jax.sharding import PartitionSpec as P

MESH = pl.DeviceIdType.MESH
F32 = jnp.float32
BF16 = jnp.bfloat16
I32 = jnp.int32


NEAR = sorted((d for d in range(1, 16)), key=lambda d: min(d // 4, 4 - d // 4) + min(d % 4, 4 - d % 4))
FAR = NEAR[::-1]
RING = sorted(range(1, 16), key=lambda d: -min(d, 16 - d))


def other(ep, d):
    y, x = lax.div(ep, 4), lax.rem(ep, 4)
    return lax.rem(y + d // 4, 4) * 4 + lax.rem(x + d % 4, 4)


def iota(shape, dim):
    return lax.broadcasted_iota(I32, shape, dim)


def one(cond):
    return jnp.where(cond, 1.0, 0.0).astype(BF16)


def mm(a, b):
    return jnp.dot(a, b, preferred_element_type=F32)


def gelu(x):
    return 0.5 * x * (1.0 + lax.erf(x * (2.0 ** -0.5)))


def compact(ch, sc, cap):
    nb = cap // 128
    na = 16 * nb
    own = lax.shift_right_logical(ch, 14)
    row = ch & 16383
    rep = one((iota((16, 256), 1) & 15) == iota((16, 256), 0))
    ownrep = mm(own.astype(F32).astype(BF16), rep)
    hit = ownrep == lax.shift_right_logical(iota((64, 256), 1), 4).astype(F32)
    hits = one(hit)
    before = mm(one(iota((64, 64), 1) < iota((64, 64), 0)), hits)
    total = mm(jnp.ones((8, 64), BF16), hits)
    r2, c2 = iota((256, 256), 0), iota((256, 256), 1)
    step = one((lax.shift_right_logical(r2, 4) == lax.shift_right_logical(c2, 4)) & ((r2 & 15) < (c2 & 15)))
    start = mm(total.astype(BF16), step)
    over = jnp.max(jnp.where(start + total > float(cap), 1.0, 0.0), axis=1, keepdims=True)[0:1]
    place = jnp.where(hit, before + start[0:1], 0.0).astype(I32)
    fold = one((iota((256, 16), 0) & 15) == iota((256, 16), 1))
    low = mm((place & 255).astype(F32).astype(BF16), fold)
    high = mm(lax.shift_right_logical(place, 8).astype(F32).astype(BF16), fold)
    rank = (low + 256.0 * high).astype(I32)
    line = own * nb + lax.shift_right_logical(rank, 7)
    line = jnp.where(rank < cap, line, -1)
    lane = rank & 127
    top = jnp.max(sc, axis=1, keepdims=True)
    ex = jnp.exp(sc - top)
    gate = ex / jnp.sum(ex, axis=1, keepdims=True)
    wide = jnp.concatenate(
        [line.astype(F32), row.astype(F32), gate, jnp.zeros((64, 80), F32)], axis=1)
    wide = jnp.concatenate([wide, jnp.zeros((64, 128), F32)], axis=0)
    turned = wide.T

    def two(x):
        return jnp.concatenate([x[0:8, 0:64], x[8:16, 0:64]], axis=1)

    line_t = two(turned[0:16]).astype(I32)
    row_t = two(turned[16:32]).astype(I32)
    gate_t = two(turned[32:48])
    g1 = gate_t.astype(BF16).astype(F32)
    g2 = (gate_t - g1).astype(BF16).astype(F32)
    g3 = gate_t - g1 - g2
    token = lax.shift_right_logical(iota((8, 128), 1) & 63, 2)
    pieces = (
        (row_t & 255).astype(F32),
        (lax.shift_right_logical(row_t, 8) & 31).astype(F32),
        (lax.shift_right_logical(row_t, 13) * 16 + token).astype(F32),
        g1, g2, g3,
    )
    lane2 = jnp.concatenate([lane[:, 0:8], lane[:, 8:16]], axis=0)
    lefts, rights = [], []
    for k in range(8):
        at = iota((na, 128), 0) == line_t[k : k + 1]
        lefts.append(jnp.concatenate([jnp.where(at, p[k : k + 1], 0.0) for p in pieces], axis=0).astype(BF16))
        rights.append(one(iota((128, 128), 1) == lane2[:, k : k + 1]))
    got = mm(jnp.concatenate(lefts, axis=1), jnp.concatenate(rights, axis=0))
    rows = got[0:na] + 256.0 * got[na : 2 * na]
    sels = got[2 * na : 3 * na]
    gates = got[3 * na : 4 * na] + got[4 * na : 5 * na] + got[5 * na : 6 * na]
    return rows, sels, gates, over


def kernel(cap, feat, key_hbm, val_hbm, chosen_hbm, scores_hbm, out, flag,
           chosen, scores, keys, vals, table, msg, got, feats, fplace, idx_v, idx_s, sel_v, gate_v, picked,
           part, pair, half, zbuf, wbuf, wvec, obuf, dbuf,
           in_sem, idx_sem, a_send, a_recv, f_send, f_recv, p_send, p_recv, z_send, z_recv, w_send, w_recv, d_send, d_recv):
    nb = cap // 128
    nq = 16 * nb
    nh = nq // 2
    ep, tp = lax.axis_index("ep"), lax.axis_index("tp")
    core, z = lax.rem(tp, 2), lax.div(tp, 2)
    mate = tp + 1 - 2 * core

    ins = [pltpu.make_async_copy(a, b, in_sem.at[k]) for k, (a, b) in enumerate(
        ((chosen_hbm, chosen), (scores_hbm, scores), (key_hbm, keys), (val_hbm, vals)))]
    for c in ins:
        c.start()

    barrier = pltpu.get_barrier_semaphore()
    for d in RING:
        pl.semaphore_signal(barrier, inc=1, device_id=(ep, lax.rem(tp + 2 * d, 32)), device_id_type=MESH)
    for d in FAR:
        pl.semaphore_signal(barrier, inc=1, device_id=(other(ep, d), tp), device_id_type=MESH)
    pl.semaphore_signal(barrier, inc=1, device_id=(ep, mate), device_id_type=MESH)

    ins[0].wait()
    ins[1].wait()
    rows, sels, gates, over = compact(chosen[...], scores[...], cap)
    for e in range(16):
        msg[e, 0:nb] = rows[e * nb : (e + 1) * nb]
        msg[e, nb : 2 * nb] = sels[e * nb : (e + 1) * nb]
        msg[e, 2 * nb : 3 * nb] = gates[e * nb : (e + 1) * nb]
        msg[e, 3 * nb : 3 * nb + 1] = jnp.broadcast_to(over, (1, 128))

    def list_copy(d):
        e = other(ep, d)
        return pltpu.make_async_remote_copy(
            src_ref=msg.at[e], dst_ref=got.at[ep], send_sem=a_send.at[d], recv_sem=a_recv.at[d],
            device_id=(e, tp), device_id_type=MESH)

    def feat_copy(d):
        e = other(ep, d)
        return pltpu.make_async_remote_copy(
            src_ref=feat, dst_ref=feats.at[ep], send_sem=f_send.at[d], recv_sem=f_recv.at[d],
            device_id=(e, tp), device_id_type=MESH)

    pl.semaphore_wait(barrier, 31)
    for d in FAR:
        list_copy(d).start()
    for d in FAR:
        feat_copy(d).start()
    got[ep] = msg[ep]
    feats[ep] = feat[...]
    ins[2].wait()
    ins[3].wait()

    def turn(b, _):
        at = pl.multiple_of(b * 128, 128)
        block = jnp.concatenate(
            [keys[:, pl.ds(at, 128)], vals[:, pl.ds(at, 128)],
             keys[:, pl.ds(at + 8192, 128)], vals[:, pl.ds(at + 8192, 128)]], axis=0).astype(F32)
        table[pl.ds(at, 128), :] = block.T
        return 0

    lax.fori_loop(0, 64, turn, 0)

    for d in NEAR:
        list_copy(d).wait_recv()
    for s in range(16):
        idx_v[s * nb : (s + 1) * nb] = got[s, 0:nb].astype(I32)

    def idx_copy(q):
        return pltpu.make_async_copy(idx_v.at[q], idx_s.at[pl.ds(q * 128, 128)], idx_sem.at[q])

    worst = got[0, 3 * nb : 3 * nb + 1]
    for s in range(16):
        sel_v[s * nb : (s + 1) * nb] = got[s, nb : 2 * nb].astype(I32)
        gate_v[s * nb : (s + 1) * nb] = got[s, 2 * nb : 3 * nb]
        if s:
            worst = jnp.maximum(worst, got[s, 3 * nb : 3 * nb + 1])
    for q in range(nq):
        idx_copy(q).start()
    for d in NEAR:
        feat_copy(d).wait_recv()
    flag[0, 0] = jnp.max(worst).astype(I32)
    place0 = one(iota((32, 128), 0) == iota((32, 128), 1))
    place1 = one(iota((32, 128), 0) + 64 == iota((32, 128), 1))
    for s in range(16):
        f = feats[s]
        fplace[s, 0:16] = mm(f, place0).astype(BF16)
        fplace[s, 16:32] = mm(f, place1).astype(BF16)
    for q in range(nq):
        idx_copy(q).wait()

    def gather(g, _):
        base = pl.multiple_of(g * 16, 16)
        for j in range(16):
            r = idx_s[base + j] & 8191
            picked[pl.ds(base + j, 1), :] = table[pl.ds(r, 1), :]
        return 0

    lax.fori_loop(0, nq * 8, gather, 0)

    def dots(g, _):
        for j in range(8):
            q = g * 8 + j
            f = fplace[lax.div(q, nb)]
            rows_q = picked[pl.ds(pl.multiple_of(q * 128, 128), 128), :].astype(BF16)
            all_q = lax.dot_general(f, rows_q, (((1,), (1,)), ((), ())), preferred_element_type=F32)
            mine = iota((32, 128), 0) == sel_v[pl.ds(q, 1), :]
            part[pl.ds(q, 1), :] = jnp.sum(jnp.where(mine, all_q, 0.0), axis=0, keepdims=True)
        return 0

    lax.fori_loop(0, nq // 8, dots, 0)

    mine_at = pl.multiple_of(core * nh, 8)
    theirs_at = pl.multiple_of((1 - core) * nh, 8)
    pair_copy = pltpu.make_async_remote_copy(
        src_ref=part.at[pl.ds(theirs_at, nh)], dst_ref=pair, send_sem=p_send, recv_sem=p_recv,
        device_id=(ep, mate), device_id_type=MESH)
    pair_copy.start()
    pair_copy.wait_recv()
    half[...] = (part[pl.ds(mine_at, nh), :] + pair[...]).astype(BF16)

    def z_copy(d):
        return pltpu.make_async_remote_copy(
            src_ref=half, dst_ref=zbuf.at[z], send_sem=z_send.at[d], recv_sem=z_recv.at[d],
            device_id=(ep, lax.rem(tp + 2 * d, 32)), device_id_type=MESH)

    for d in RING:
        z_copy(d).start()
    zbuf[z] = half[...]
    for d in RING:
        z_copy(d).wait_recv()
    whole = zbuf[0].astype(F32)
    for k in range(1, 16):
        whole = whole + zbuf[k].astype(F32)
    wbuf[core] = (gate_v[pl.ds(mine_at, nh), :] * gelu(whole)).astype(BF16)
    w_copy = pltpu.make_async_remote_copy(
        src_ref=wbuf.at[core], dst_ref=wbuf.at[core], send_sem=w_send, recv_sem=w_recv,
        device_id=(ep, mate), device_id_type=MESH)
    w_copy.start()
    w_copy.wait_recv()
    wvec[0:nh] = wbuf[0].astype(F32)
    wvec[nh:nq] = wbuf[1].astype(F32)

    def out_copy(d):
        s = other(ep, d)
        return pltpu.make_async_remote_copy(
            src_ref=obuf.at[s], dst_ref=dbuf.at[ep], send_sem=d_send.at[d], recv_sem=d_recv.at[d],
            device_id=(s, tp), device_id_type=MESH)

    for s in range(16):
        acc = None
        for j in range(nb):
            q = s * nb + j
            mine = iota((32, 128), 0) == sel_v[q : q + 1]
            spread = jnp.where(mine, wvec[q : q + 1], 0.0).astype(BF16)
            term = mm(spread, picked[q * 128 : (q + 1) * 128].astype(BF16))
            acc = term if acc is None else acc + term
        obuf[s] = acc[0:16] + pltpu.roll(acc[16:32], 64, 1)
    for d in FAR:
        out_copy(d).start()
    dbuf[ep] = obuf[ep]
    for d in NEAR:
        out_copy(d).wait_recv()
    full = dbuf[0]
    for k in range(1, 16):
        full = full + dbuf[k]
    out[...] = pltpu.roll(full, 96, 1)[:, 0:32].astype(BF16)

    for d in NEAR:
        list_copy(d).wait_send()
        feat_copy(d).wait_send()
        z_copy(d).wait_send()
        out_copy(d).wait_send()
    pair_copy.wait_send()
    w_copy.wait_send()


def run(cap, cid, feat, key_t, val_t, chosen, scores):
    nb = cap // 128
    nq = 16 * nb
    nh = nq // 2
    mr = (3 * nb + 1 + 7) // 8 * 8
    dma = pltpu.SemaphoreType.DMA
    vmem = pltpu.VMEM
    return pl.pallas_call(
        functools.partial(kernel, cap),
        out_shape=(jax.ShapeDtypeStruct((16, 32), BF16), jax.ShapeDtypeStruct((1, 1), I32)),
        in_specs=[pl.BlockSpec(memory_space=vmem), pl.BlockSpec(memory_space=pl.ANY), pl.BlockSpec(memory_space=pl.ANY),
                  pl.BlockSpec(memory_space=pl.ANY), pl.BlockSpec(memory_space=pl.ANY)],
        out_specs=(pl.BlockSpec(memory_space=vmem), pl.BlockSpec(memory_space=pltpu.SMEM)),
        scratch_shapes=[
            vmem((64, 16), I32), vmem((64, 16), F32), vmem((32, 16384), BF16), vmem((32, 16384), BF16), vmem((8192, 128), F32),
            vmem((16, mr, 128), F32), vmem((16, mr, 128), F32), vmem((16, 16, 32), BF16), vmem((16, 32, 128), BF16),
            vmem((nq, 128), I32), pltpu.SMEM((nq * 128,), I32), vmem((nq, 128), I32), vmem((nq, 128), F32),
            vmem((nq * 128, 128), F32),
            vmem((nq, 128), F32), vmem((nh, 128), F32), vmem((nh, 128), BF16), vmem((16, nh, 128), BF16),
            vmem((2, nh, 128), BF16), vmem((nq, 128), F32), vmem((16, 16, 128), F32), vmem((16, 16, 128), F32),
            dma((4,)), dma((nq,)), dma((16,)), dma((16,)), dma((16,)), dma((16,)), dma, dma, dma((16,)), dma((16,)), dma, dma,
            dma((16,)), dma((16,)),
        ],
        compiler_params=pltpu.CompilerParams(collective_id=cid, has_side_effects=True, vmem_limit_bytes=48 << 20),
    )(feat, key_t, val_t, chosen, scores)


def blocks(func, arrays):
    split = tuple(x.reshape((8, 32) + x.shape[1:]) for x in arrays)
    done = lax.map(func, split)
    return done.reshape((256,) + done.shape[2:])


def dense(features, key_table, value_table, chosen, scores):
    first = lax.axis_index("ep") * 16384
    every = lax.all_gather(chosen, "ep", axis=0, tiled=True)
    gates = lax.all_gather(jax.nn.softmax(scores, axis=-1), "ep", axis=0, tiled=True).reshape(256, 64)
    tokens = lax.all_gather(features, "ep", axis=0, tiled=True)
    shifted = every.reshape(256, 64) - first
    owned = (shifted >= 0) & (shifted < 16384)
    rows = jnp.clip(shifted, 0, 16383)

    def dots(pair):
        block, at = pair
        full = lax.dot_general(block, key_table, (((1,), (1,)), ((), ())), preferred_element_type=F32)
        return jnp.take_along_axis(full, at, axis=1)

    partial = jnp.where(owned, blocks(dots, (tokens, rows)), 0.0)
    products = jnp.concatenate(
        [lax.all_gather(partial[k * 64 : (k + 1) * 64], "tp").sum(0) for k in range(4)], axis=0)
    weights = (gates * jax.nn.gelu(products, approximate=False)).astype(BF16)
    weights = jnp.where(owned, weights, jnp.zeros_like(weights))

    def spread(pair):
        block, at = pair
        ids = lax.broadcasted_iota(I32, at.shape, 0)
        full = jnp.zeros((32, 16384), F32).at[ids, at].add(block.astype(F32))
        upper = full.astype(BF16)
        lower = (full - upper.astype(F32)).astype(BF16)
        return mm(upper, value_table) + mm(lower, value_table)

    terms = lax.all_gather(blocks(spread, (weights, rows)), "ep").sum(0)
    return lax.dynamic_slice_in_dim(terms, lax.axis_index("ep") * 16, 16, 0).astype(BF16)


def local(features, key_table, value_table, chosen, scores):
    quick, flag = run(256, 0, features, key_table.T, value_table.T, chosen.reshape(64, 16), scores.reshape(64, 16))
    return lax.cond(flag[0, 0] > 0, lambda: dense(features, key_table, value_table, chosen, scores), lambda: quick)


def solution(mesh):
    spec = P("ep", "tp")
    whole = P("ep", None, None)
    return jax.shard_map(local, mesh=mesh, in_specs=(spec, spec, spec, whole, whole), out_specs=spec, check_vma=False)
```

time: 518 us -> 49.1 us (0.09)
  local copies, waits for them, and re-layouts: 159 us -> 0.61 us
  other arithmetic: 142 us -> 0 us
  waiting for transfers between devices: 104 us -> 0 us
  blocking collectives: 84.1 us -> 0 us
  Pallas kernels: 0 us -> 47.3 us
  between operations: 13.3 us -> 0.77 us
  matrix products: 10.1 us -> 0 us
    while x32 -> x0, other arithmetic: 135 us -> none
    gather x24 -> x0, local copies, waits for them, and re-layouts: 134 us -> none  [dots_block(): return jnp.take_along_axis(dense, picked, axis=1)]
    all_gather x1 -> x0, waiting for transfers between devices: 66.9 us -> none  [over_pieces(): return lax.all_gather(shard, axis).sum(0)]
    all_gather x4 -> x0, blocking collectives: 56.6 us -> none  [the longest x2 21 us: gathered_by_axis(): nearer = lax.all_gather(shard, axes[-1], axis=dim, tiled=True)]
    pallas_call x0 -> x1, Pallas kernels: none -> 47.3 us  [run(): pl.pallas_call(functools.partial(kernel, cap), out_shape=(jax.ShapeDtypeS...]
    reduce_scatter x2 -> x0, waiting for transfers between devices: 36.6 us -> none  [reduced_to_own(): blocks = lax.psum_scatter(blocks, axes[k], scatter_dimension=0, tiled=True)]
    unnamed x2 -> x0, blocking collectives: 27.5 us -> none
    scatter-add x8 -> x0, local copies, waits for them, and re-layouts: 14 us -> none  [value_block(): dense = jnp.zeros((width, table_rows), jnp.float32).at[token_ids, picked]...]
  transfers between devices with their start and end apart: 3 -> 0, of which waited for: 3 -> 0; matrix products, arithmetic and copies ran while one was open for 1% -> 0% of each run, Pallas kernels for 0% -> 0%
where the time goes in v1:
time: 49.1 us; the launch traced here: 48.9 us
  Pallas kernels  47.3 us (96%)
  between operations  0.77 us (2%)
  local copies, waits for them, and re-layouts  0.61 us (1%)
    pallas_call x1, Pallas kernels, run(): pl.pallas_call(functools.partial(kernel, cap), out_shape=(jax.ShapeDtypeS...  47.3 us

profile of v1, /device:TPU:1, one launch (start us, length us, event | category | flops | bytes accessed | tf_op | source)
XLA Modules:
  0.0 48.9 jit_solution(5672895497249674715)
XLA Ops:
  0.0 0.0 copy-start.1
  0.0 0.0 copy-start.2
  0.0 0.0 copy-start.3
  0.0 0.0 copy-start.4
  0.0 0.0 copy-start.5
  0.0 47.3 %shard_map.57 = (bf16[16,32]{1,0:T(8,128)(2,1)S(1)}, s32[1,1]{1,0:T(1,128)}) custom-call(bf16[16,32]{1,0:T(8,128)(2,1)} %feat.1, bf16[32,16384]{1,0:T(8,128)(2,1)} %bitcast.58, bf16[32,16384]{1,0:T(8,128)(2,1)} %bitcast.59, s32[64,16]{1,0:T(8,128)} %bitcast.67, f32[64,16]{1,0:T(8,128)} %bitcast.70), custom_call_target="tpu_custom_call" | custom-call | tf_op jit(solution)/shard_map/pallas_call | solution.py:287
  48.0 0.0 copy-done.1
  48.1 0.0 copy-done.2
  48.1 0.0 copy-done.3
  48.1 0.0 copy-done.4
  48.1 0.0 copy-done.5
  48.1 0.2 conditional.1
  48.3 0.6 %copy.135 = bf16[16,32]{1,0:T(8,128)(2,1)} copy(bf16[16,32]{1,0:T(8,128)(2,1)S(1)} %get-tuple-element.163) | data formatting | bytes 2048
Async XLA Ops:
  0.0 48.0 %copy-start.1 = (bf16[16384,32]{0,1:T(8,128)(2,1)S(1)}, bf16[16384,32]{0,1:T(8,128)(2,1)}, u32[]{:S(2)}) copy-start(bf16[16384,32]{0,1:T(8,128)(2,1)} %param.12) | copy-start | bytes 3145732
  0.0 48.1 %copy-start.2 = (bf16[16384,32]{0,1:T(8,128)(2,1)S(1)}, bf16[16384,32]{0,1:T(8,128)(2,1)}, u32[]{:S(2)}) copy-start(bf16[16384,32]{0,1:T(8,128)(2,1)} %param.13) | copy-start | bytes 3145732
  0.0 48.1 %copy-start.3 = (s32[16,4,16]{2,1,0:T(4,128)S(1)}, s32[16,4,16]{2,1,0:T(4,128)}, u32[]{:S(2)}) copy-start(s32[16,4,16]{2,1,0:T(4,128)} %param.14) | copy-start | bytes 12292
  0.0 48.1 %copy-start.4 = (f32[16,4,16]{2,1,0:T(4,128)S(1)}, f32[16,4,16]{2,1,0:T(4,128)}, u32[]{:S(2)}) copy-start(f32[16,4,16]{2,1,0:T(4,128)} %param.15) | copy-start | bytes 12292
  0.0 48.1 %copy-start.5 = (bf16[16,32]{1,0:T(8,128)(2,1)S(1)}, bf16[16,32]{1,0:T(8,128)(2,1)}, u32[]{:S(2)}) copy-start(bf16[16,32]{1,0:T(8,128)(2,1)} %feat.1) | copy-start | bytes 3076

commit v2 on v1

v2 whole, which is shorter than its diff:
```python
import functools

import jax
import jax.numpy as jnp
from jax import lax
from jax.experimental import pallas as pl
from jax.experimental.pallas import tpu as pltpu
from jax.sharding import PartitionSpec as P

MESH = pl.DeviceIdType.MESH
F32 = jnp.float32
BF16 = jnp.bfloat16
I32 = jnp.int32


def hops(d):
    return min(d // 4, 4 - d // 4) + min(d % 4, 4 - d % 4)


ORDER = sorted(range(16), key=hops)
BACK = [(-(d // 4)) % 4 * 4 + (-(d % 4)) % 4 for d in ORDER]
RING = sorted(range(1, 16), key=lambda d: -min(d, 16 - d))


def other(ep, d):
    y, x = lax.div(ep, 4), lax.rem(ep, 4)
    return lax.rem(y + d // 4, 4) * 4 + lax.rem(x + d % 4, 4)


def iota(shape, dim):
    return lax.broadcasted_iota(I32, shape, dim)


def one(cond):
    return jnp.where(cond, 1.0, 0.0).astype(BF16)


def mm(a, b):
    return jnp.dot(a, b, preferred_element_type=F32)


def gelu(x):
    return 0.5 * x * (1.0 + lax.erf(x * (2.0 ** -0.5)))


def compact(ch, sc, cap):
    nb = cap // 128
    na = 16 * nb
    own = lax.shift_right_logical(ch, 14)
    row = ch & 16383
    rep = one((iota((16, 256), 1) & 15) == iota((16, 256), 0))
    ownrep = mm(own.astype(F32).astype(BF16), rep)
    hit = ownrep == lax.shift_right_logical(iota((64, 256), 1), 4).astype(F32)
    hits = one(hit)
    before = mm(one(iota((64, 64), 1) < iota((64, 64), 0)), hits)
    total = mm(jnp.ones((8, 64), BF16), hits)
    r2, c2 = iota((256, 256), 0), iota((256, 256), 1)
    step = one((lax.shift_right_logical(r2, 4) == lax.shift_right_logical(c2, 4)) & ((r2 & 15) < (c2 & 15)))
    start = mm(total.astype(BF16), step)
    over = jnp.max(jnp.where(start + total > float(cap), 1.0, 0.0), axis=1, keepdims=True)[0:1]
    place = jnp.where(hit, before + start[0:1], 0.0).astype(I32)
    fold = one((iota((256, 16), 0) & 15) == iota((256, 16), 1))
    low = mm((place & 255).astype(F32).astype(BF16), fold)
    high = mm(lax.shift_right_logical(place, 8).astype(F32).astype(BF16), fold)
    rank = (low + 256.0 * high).astype(I32)
    line = own * nb + lax.shift_right_logical(rank, 7)
    line = jnp.where(rank < cap, line, -1)
    lane = rank & 127
    top = jnp.max(sc, axis=1, keepdims=True)
    ex = jnp.exp(sc - top)
    gate = ex / jnp.sum(ex, axis=1, keepdims=True)
    wide = jnp.concatenate(
        [line.astype(F32), row.astype(F32), gate, jnp.zeros((64, 80), F32)], axis=1)
    wide = jnp.concatenate([wide, jnp.zeros((64, 128), F32)], axis=0)
    turned = wide.T

    def two(x):
        return jnp.concatenate([x[0:8, 0:64], x[8:16, 0:64]], axis=1)

    line_t = two(turned[0:16]).astype(I32)
    row_t = two(turned[16:32]).astype(I32)
    gate_t = two(turned[32:48])
    g1 = gate_t.astype(BF16).astype(F32)
    g2 = (gate_t - g1).astype(BF16).astype(F32)
    g3 = gate_t - g1 - g2
    token = lax.shift_right_logical(iota((8, 128), 1) & 63, 2)
    pieces = (
        (row_t & 255).astype(F32),
        (lax.shift_right_logical(row_t, 8) & 31).astype(F32),
        (lax.shift_right_logical(row_t, 13) * 16 + token).astype(F32),
        g1, g2, g3,
    )
    lane2 = jnp.concatenate([lane[:, 0:8], lane[:, 8:16]], axis=0)
    lefts, rights = [], []
    for k in range(8):
        at = iota((na, 128), 0) == line_t[k : k + 1]
        lefts.append(jnp.concatenate([jnp.where(at, p[k : k + 1], 0.0) for p in pieces], axis=0).astype(BF16))
        rights.append(one(iota((128, 128), 1) == lane2[:, k : k + 1]))
    got = mm(jnp.concatenate(lefts, axis=1), jnp.concatenate(rights, axis=0))
    codes = got[0:na] + 256.0 * got[na : 2 * na] + 8192.0 * got[2 * na : 3 * na] + 262144.0 * over
    gates = got[3 * na : 4 * na] + got[4 * na : 5 * na] + got[5 * na : 6 * na]
    return codes, gates


def packed(f):
    lanes = mm(f, one(iota((32, 128), 0) == (iota((32, 128), 1) & 31)))
    keep = lax.shift_right_logical(iota((16, 128), 0), 2) == lax.shift_right_logical(iota((16, 128), 1), 5)
    lanes = jnp.where(keep, lanes, 0.0)
    return lanes[0:4] + lanes[4:8] + lanes[8:12] + lanes[12:16]


def kernel(cap, feat_hbm, key_hbm, val_hbm, chosen_hbm, scores_hbm, out, flag,
           feat, chosen, scores, keys, vals, table, msg, got, fplace, idx_v, idx_s, sel_v, gate_v, picked,
           part, pair, half, zbuf, wbuf, wvec, obuf, dbuf,
           in_sem, idx_sem, a_send, a_recv, p_send, p_recv, z_send, z_recv, w_send, w_recv, d_send, d_recv, known):
    nb = cap // 128
    nh = 8 * nb
    ep, tp = lax.axis_index("ep"), lax.axis_index("tp")
    core, z = lax.rem(tp, 2), lax.div(tp, 2)
    mate = tp + 1 - 2 * core

    ins = [pltpu.make_async_copy(a, b, in_sem.at[k]) for k, (a, b) in enumerate(
        ((chosen_hbm, chosen), (scores_hbm, scores), (feat_hbm, feat), (key_hbm, keys), (val_hbm, vals)))]
    for c in ins:
        c.start()

    def along(d):
        return (ep, lax.rem(tp + 2 * d + 32, 32))

    def tell(sem, d):
        pl.semaphore_signal(sem, inc=1, device_id=along(d), device_id_type=MESH)
        pl.semaphore_signal(sem, inc=1, device_id=along(-d), device_id_type=MESH)

    barrier = pltpu.get_barrier_semaphore()
    for p in range(15, 0, -1):
        pl.semaphore_signal(barrier, inc=1, device_id=(other(ep, ORDER[p]), tp), device_id_type=MESH)
    tell(barrier, 1)
    pl.semaphore_signal(barrier, inc=1, device_id=(ep, mate), device_id_type=MESH)

    for c in ins[:3]:
        c.wait()
    codes, gates = compact(chosen[...], scores[...], cap)
    tokens = packed(feat[...])
    for e in range(16):
        msg[e, 0:nb] = codes[e * nb : (e + 1) * nb]
        msg[e, nb : 2 * nb] = gates[e * nb : (e + 1) * nb]
        msg[e, 2 * nb : 2 * nb + 4] = tokens

    def list_copy(p):
        e = other(ep, BACK[p])
        return pltpu.make_async_remote_copy(
            src_ref=msg.at[e], dst_ref=got.at[p % 2, p // 2], send_sem=a_send.at[p], recv_sem=a_recv.at[p],
            device_id=(e, tp), device_id_type=MESH)

    pl.semaphore_wait(barrier, 18)
    for p in range(15, 0, -1):
        list_copy(p).start()
    tell(known.at[0], 1)
    got[0, 0] = msg[ep]
    ins[3].wait()
    ins[4].wait()

    same = one(iota((128, 128), 0) == iota((128, 128), 1))

    def turn(b, _):
        for j in range(4):
            at = pl.multiple_of(b * 512 + j * 128, 128)
            block = jnp.concatenate(
                [keys[:, pl.ds(at, 128)], vals[:, pl.ds(at, 128)],
                 keys[:, pl.ds(at + 8192, 128)], vals[:, pl.ds(at + 8192, 128)]], axis=0)
            table[pl.ds(at, 128), :] = lax.dot_general(
                same, block, (((1,), (1,)), ((), ())), preferred_element_type=F32)
        return 0

    lax.fori_loop(0, 16, turn, 0)
    pl.semaphore_wait(known.at[0], 2)
    tell(known.at[1], 2)

    r2, c2 = iota((128, 256), 0), iota((128, 256), 1)
    fold = one((c2 & 127) - 64 * lax.shift_right_logical(c2, 7) == (r2 & 31))
    keep = lax.shift_right_logical(iota((16, 128), 0), 2) == lax.shift_right_logical(iota((16, 128), 1), 5)

    def idx_copy(h, r):
        row = h * nh + r
        return pltpu.make_async_copy(idx_v.at[h, r], idx_s.at[pl.ds(row * 128, 128)], idx_sem.at[row])

    def arrive(slots):
        for h, m in slots:
            if not (m == 0 and isinstance(h, int) and h == 0):
                pltpu.make_async_remote_copy(
                    src_ref=msg.at[0], dst_ref=got.at[h, m], send_sem=a_send.at[0], recv_sem=a_recv.at[2 * m + h],
                    device_id=(ep, mate), device_id_type=MESH).wait_recv()
        for h, m in slots:
            at = slice(m * nb, (m + 1) * nb)
            code = got[h, m, 0:nb].astype(I32)
            idx_v[h, at] = code & 8191
            sel_v[h, at] = lax.shift_right_logical(code, 13) & 31
            gate_v[h, at] = got[h, m, nb : 2 * nb]
        for h, m in slots:
            f = got[h, m, 2 * nb : 2 * nb + 4]
            f = jnp.where(keep, jnp.concatenate([f, f, f, f], axis=0), 0.0).astype(BF16)
            f = mm(f, fold).astype(BF16)
            fplace[h, m, 0:16] = f[:, 0:128]
            fplace[h, m, 16:32] = f[:, 128:256]
        for h, m in slots:
            for j in range(nb):
                idx_copy(h, m * nb + j).start()

    def fetch(slots, runs):
        for h, m in slots:
            for j in range(nb):
                idx_copy(h, m * nb + j).wait()
        for h, m, n in runs:
            first = (h * 8 + m) * cap

            def gather(g, _):
                base = pl.multiple_of(first + g * 16, 16)
                for j in range(16):
                    r = idx_s[base + j] & 8191
                    picked[pl.ds(base + j, 1), :] = table[pl.ds(r, 1), :]
                return 0

            lax.fori_loop(0, n * cap // 16, gather, 0)
        for h, m in slots:
            for j in range(nb):
                r = m * nb + j
                rows_q = picked[pl.ds(pl.multiple_of((h * nh + r) * 128, 128), 128), :].astype(BF16)
                all_q = lax.dot_general(fplace[h, m], rows_q, (((1,), (1,)), ((), ())), preferred_element_type=F32)
                mine = iota((32, 128), 0) == sel_v[h, r : r + 1]
                part[h, r : r + 1] = jnp.sum(jnp.where(mine, all_q, 0.0), axis=0, keepdims=True)

    g0 = [(0, 0), (1, 0), (0, 1), (1, 1)]
    g1 = [(0, 2), (1, 2), (0, 3), (1, 3)]
    g2 = [(1 - core, m) for m in range(4, 8)]
    g3 = [(core, m) for m in range(4, 8)]
    arrive(g0)
    arrive(g1)
    pl.semaphore_wait(known.at[1], 2)
    tell(known.at[2], 4)
    fetch(g0, [(0, 0, 2), (1, 0, 2)])
    arrive(g2)
    fetch(g1, [(0, 2, 2), (1, 2, 2)])
    arrive(g3)
    fetch(g2, [(1 - core, 4, 4)])
    pair_copy = pltpu.make_async_remote_copy(
        src_ref=part.at[1 - core], dst_ref=pair, send_sem=p_send, recv_sem=p_recv,
        device_id=(ep, mate), device_id_type=MESH)
    pair_copy.start()
    fetch(g3, [(core, 4, 4)])
    pl.semaphore_wait(known.at[2], 2)
    pair_copy.wait_recv()
    half[...] = (part[core] + pair[...]).astype(BF16)

    def z_copy(d):
        return pltpu.make_async_remote_copy(
            src_ref=half, dst_ref=zbuf.at[z], send_sem=z_send.at[d], recv_sem=z_recv.at[d],
            device_id=along(d), device_id_type=MESH)

    for d in RING:
        z_copy(d).start()
    zbuf[z] = half[...]
    worst = got[0, 0, 0:nb]
    for p in range(1, 16):
        worst = jnp.maximum(worst, got[p % 2, p // 2, 0:nb])
    flag[0, 0] = lax.shift_right_logical(jnp.max(worst).astype(I32), 18)
    for d in RING:
        z_copy(d).wait_recv()
    whole = zbuf[0].astype(F32)
    for k in range(1, 16):
        whole = whole + zbuf[k].astype(F32)
    weights = (gate_v[core] * gelu(whole)).astype(BF16)
    wbuf[core] = weights
    wvec[core] = weights.astype(F32)
    w_copy = pltpu.make_async_remote_copy(
        src_ref=wbuf.at[core], dst_ref=wbuf.at[core], send_sem=w_send, recv_sem=w_recv,
        device_id=(ep, mate), device_id_type=MESH)
    w_copy.start()

    group = lax.shift_right_logical(iota((4, 128), 1), 5)

    def sums(h):
        for m in range(8):
            acc = None
            for j in range(nb):
                r = m * nb + j
                mine = iota((32, 128), 0) == sel_v[h, r : r + 1]
                spread = jnp.where(mine, wvec[h, r : r + 1], 0.0).astype(BF16)
                rows_q = picked[pl.ds(pl.multiple_of((h * nh + r) * 128, 128), 128), :].astype(BF16)
                term = mm(spread, rows_q)
                acc = term if acc is None else acc + term
            block = acc[0:16] + pltpu.roll(acc[16:32], 64, 1)
            top, low = block[0:8], block[8:16]
            obuf[2 * m + h] = jnp.where(
                group == 0, pltpu.roll(top, 96, 1)[0:4],
                jnp.where(group == 1, top[4:8],
                          jnp.where(group == 2, pltpu.roll(low, 32, 1)[0:4], pltpu.roll(low, 64, 1)[4:8])))

    def out_copy(h, m):
        p = 2 * m + h
        y = ORDER[2 * m] // 4 + h * (ORDER[2 * m + 1] // 4 - ORDER[2 * m] // 4)
        x = ORDER[2 * m] % 4 + h * (ORDER[2 * m + 1] % 4 - ORDER[2 * m] % 4)
        s = lax.rem(lax.div(ep, 4) + y, 4) * 4 + lax.rem(lax.rem(ep, 4) + x, 4)
        return pltpu.make_async_remote_copy(
            src_ref=obuf.at[p], dst_ref=dbuf.at[p], send_sem=d_send.at[p], recv_sem=d_recv.at[p],
            device_id=(s, tp), device_id_type=MESH)

    sums(core)
    for m in range(7, 0, -1):
        out_copy(core, m).start()
    w_copy.wait_recv()
    wvec[1 - core] = wbuf[1 - core].astype(F32)
    sums(1 - core)
    for m in range(7, 0, -1):
        out_copy(1 - core, m).start()
    out_copy(1, 0).start()
    dbuf[0] = obuf[0]
    for p in range(1, 16):
        out_copy(p % 2, p // 2).wait_recv()
    full = dbuf[0]
    for p in range(1, 16):
        full = full + dbuf[p]
    full = jnp.concatenate([full, full], axis=0)
    out[...] = jnp.concatenate(
        [(pltpu.roll(full, 128 - 32 * j, 1) if j else full)[0:4, 0:32] for j in range(4)], axis=0).astype(BF16)

    for p in range(1, 16):
        list_copy(p).wait_send()
        z_copy(p).wait_send()
        out_copy(p % 2, p // 2).wait_send()
    pair_copy.wait_send()
    w_copy.wait_send()


def run(cap, cid, feat, key_t, val_t, chosen, scores):
    nb = cap // 128
    nh = 8 * nb
    dma = pltpu.SemaphoreType.DMA
    vmem = pltpu.VMEM
    return pl.pallas_call(
        functools.partial(kernel, cap),
        out_shape=(jax.ShapeDtypeStruct((16, 32), BF16), jax.ShapeDtypeStruct((1, 1), I32)),
        in_specs=[pl.BlockSpec(memory_space=pl.ANY)] * 5,
        out_specs=(pl.BlockSpec(memory_space=vmem), pl.BlockSpec(memory_space=pltpu.SMEM)),
        scratch_shapes=[
            vmem((16, 32), BF16), vmem((64, 16), I32), vmem((64, 16), F32), vmem((32, 16384), BF16), vmem((32, 16384), BF16),
            vmem((8192, 128), F32), vmem((16, 2 * nb + 4, 128), F32), vmem((2, 8, 2 * nb + 4, 128), F32),
            vmem((2, 8, 32, 128), BF16), vmem((2, nh, 128), I32), pltpu.SMEM((2 * nh * 128,), I32),
            vmem((2, nh, 128), I32), vmem((2, nh, 128), F32), vmem((2 * nh * 128, 128), F32),
            vmem((2, nh, 128), F32), vmem((nh, 128), F32), vmem((nh, 128), BF16), vmem((16, nh, 128), BF16),
            vmem((2, nh, 128), BF16), vmem((2, nh, 128), F32), vmem((16, 4, 128), F32), vmem((16, 4, 128), F32),
            dma((5,)), dma((2 * nh,)), dma((16,)), dma((16,)), dma, dma, dma((16,)), dma((16,)), dma, dma,
            dma((16,)), dma((16,)), pltpu.SemaphoreType.REGULAR((3,)),
        ],
        compiler_params=pltpu.CompilerParams(collective_id=cid, has_side_effects=True, vmem_limit_bytes=48 << 20),
    )(feat, key_t, val_t, chosen, scores)


def blocks(func, arrays):
    split = tuple(x.reshape((8, 32) + x.shape[1:]) for x in arrays)
    done = lax.map(func, split)
    return done.reshape((256,) + done.shape[2:])


def dense(features, key_table, value_table, chosen, scores):
    first = lax.axis_index("ep") * 16384
    every = lax.all_gather(chosen, "ep", axis=0, tiled=True)
    gates = lax.all_gather(jax.nn.softmax(scores, axis=-1), "ep", axis=0, tiled=True).reshape(256, 64)
    tokens = lax.all_gather(features, "ep", axis=0, tiled=True)
    shifted = every.reshape(256, 64) - first
    owned = (shifted >= 0) & (shifted < 16384)
    rows = jnp.clip(shifted, 0, 16383)

    def dots(pair):
        block, at = pair
        full = lax.dot_general(block, key_table, (((1,), (1,)), ((), ())), preferred_element_type=F32)
        return jnp.take_along_axis(full, at, axis=1)

    partial = jnp.where(owned, blocks(dots, (tokens, rows)), 0.0)
    products = jnp.concatenate(
        [lax.all_gather(partial[k * 64 : (k + 1) * 64], "tp").sum(0) for k in range(4)], axis=0)
    weights = (gates * jax.nn.gelu(products, approximate=False)).astype(BF16)
    weights = jnp.where(owned, weights, jnp.zeros_like(weights))

    def spread(pair):
        block, at = pair
        ids = lax.broadcasted_iota(I32, at.shape, 0)
        full = jnp.zeros((32, 16384), F32).at[ids, at].add(block.astype(F32))
        upper = full.astype(BF16)
        lower = (full - upper.astype(F32)).astype(BF16)
        return mm(upper, value_table) + mm(lower, value_table)

    terms = lax.all_gather(blocks(spread, (weights, rows)), "ep").sum(0)
    return lax.dynamic_slice_in_dim(terms, lax.axis_index("ep") * 16, 16, 0).astype(BF16)


def local(features, key_table, value_table, chosen, scores):
    quick, flag = run(256, 0, features, key_table.T, value_table.T, chosen.reshape(64, 16), scores.reshape(64, 16))
    return lax.cond(flag[0, 0] > 0, lambda: dense(features, key_table, value_table, chosen, scores), lambda: quick)


def solution(mesh):
    spec = P("ep", "tp")
    whole = P("ep", None, None)
    return jax.shard_map(local, mesh=mesh, in_specs=(spec, spec, spec, whole, whole), out_specs=spec, check_vma=False)
```

time: 49.1 us -> 43.6 us (0.89)
  Pallas kernels: 47.3 us -> 41.9 us
    pallas_call x1, Pallas kernels: 47.3 us -> 41.9 us  [run(): pl.pallas_call(functools.partial(kernel, cap), out_shape=(jax.ShapeDtypeS...]
where the time goes in v2:
time: 43.6 us; the launch traced here: 43.5 us
  Pallas kernels  41.9 us (96%)
  between operations  0.77 us (2%)
  local copies, waits for them, and re-layouts  0.61 us (1%)
    pallas_call x1, Pallas kernels, run(): pl.pallas_call(functools.partial(kernel, cap), out_shape=(jax.ShapeDtypeS...  41.9 us

profile of v2, /device:TPU:1, one launch (start us, length us, event | category | flops | bytes accessed | tf_op | source)
XLA Modules:
  0.0 43.5 jit_solution(942825870781932085)
XLA Ops:
  0.0 0.0 copy-start.1
  0.0 0.0 copy-start.2
  0.0 0.0 copy-start.3
  0.0 0.0 copy-start.4
  0.0 0.0 copy-start.5
  0.0 41.9 %shard_map.57 = (bf16[16,32]{1,0:T(8,128)(2,1)S(1)}, s32[1,1]{1,0:T(1,128)}) custom-call(bf16[16,32]{1,0:T(8,128)(2,1)} %feat_hbm.1, bf16[32,16384]{1,0:T(8,128)(2,1)} %bitcast.58, bf16[32,16384]{1,0:T(8,128)(2,1)} %bitcast.59, s32[64,16]{1,0:T(8,128)} %bitcast.67, f32[64,16]{1,0:T(8,128)} %bitcast.70), custom_call_target="tpu_custom_call" | custom-call | tf_op jit(solution)/shard_map/pallas_call | solution.py:339
  42.6 0.0 copy-done.1
  42.6 0.0 copy-done.2
  42.7 0.0 copy-done.3
  42.7 0.0 copy-done.4
  42.7 0.0 copy-done.5
  42.7 0.2 conditional.1
  42.9 0.6 %copy.135 = bf16[16,32]{1,0:T(8,128)(2,1)} copy(bf16[16,32]{1,0:T(8,128)(2,1)S(1)} %get-tuple-element.163) | data formatting | bytes 2048
Async XLA Ops:
  0.0 42.6 %copy-start.1 = (bf16[16384,32]{0,1:T(8,128)(2,1)S(1)}, bf16[16384,32]{0,1:T(8,128)(2,1)}, u32[]{:S(2)}) copy-start(bf16[16384,32]{0,1:T(8,128)(2,1)} %param.12) | copy-start | bytes 3145732
  0.0 42.6 %copy-start.2 = (bf16[16384,32]{0,1:T(8,128)(2,1)S(1)}, bf16[16384,32]{0,1:T(8,128)(2,1)}, u32[]{:S(2)}) copy-start(bf16[16384,32]{0,1:T(8,128)(2,1)} %param.13) | copy-start | bytes 3145732
  0.0 42.6 %copy-start.3 = (s32[16,4,16]{2,1,0:T(4,128)S(1)}, s32[16,4,16]{2,1,0:T(4,128)}, u32[]{:S(2)}) copy-start(s32[16,4,16]{2,1,0:T(4,128)} %param.14) | copy-start | bytes 12292
  0.0 42.7 %copy-start.4 = (f32[16,4,16]{2,1,0:T(4,128)S(1)}, f32[16,4,16]{2,1,0:T(4,128)}, u32[]{:S(2)}) copy-start(f32[16,4,16]{2,1,0:T(4,128)} %param.15) | copy-start | bytes 12292
  0.0 42.7 %copy-start.5 = (bf16[16,32]{1,0:T(8,128)(2,1)S(1)}, bf16[16,32]{1,0:T(8,128)(2,1)}, u32[]{:S(2)}) copy-start(bf16[16,32]{1,0:T(8,128)(2,1)} %feat_hbm.1) | copy-start | bytes 3076

commit v3 on v2

--- a/solution.py
+++ b/solution.py
@@ -115,6 +115,7 @@
            in_sem, idx_sem, a_send, a_recv, p_send, p_recv, z_send, z_recv, w_send, w_recv, d_send, d_recv, known):
     nb = cap // 128
     nh = 8 * nb
+    nw = nb // 2
     ep, tp = lax.axis_index("ep"), lax.axis_index("tp")
     core, z = lax.rem(tp, 2), lax.div(tp, 2)
     mate = tp + 1 - 2 * core
@@ -181,7 +182,7 @@
     keep = lax.shift_right_logical(iota((16, 128), 0), 2) == lax.shift_right_logical(iota((16, 128), 1), 5)
 
     def idx_copy(h, r):
-        row = h * nh + r
+        row = h * (nh // 2) + r
         return pltpu.make_async_copy(idx_v.at[h, r], idx_s.at[pl.ds(row * 128, 128)], idx_sem.at[row])
 
     def arrive(slots):
@@ -193,7 +194,7 @@
         for h, m in slots:
             at = slice(m * nb, (m + 1) * nb)
             code = got[h, m, 0:nb].astype(I32)
-            idx_v[h, at] = code & 8191
+            idx_v[h, m * nw : (m + 1) * nw] = (code[0:nw] & 8191) | lax.shift_left(code[nw:nb] & 8191, 19)
             sel_v[h, at] = lax.shift_right_logical(code, 13) & 31
             gate_v[h, at] = got[h, m, nb : 2 * nb]
         for h, m in slots:
@@ -203,24 +204,29 @@
             fplace[h, m, 0:16] = f[:, 0:128]
             fplace[h, m, 16:32] = f[:, 128:256]
         for h, m in slots:
-            for j in range(nb):
-                idx_copy(h, m * nb + j).start()
+            for j in range(nw):
+                idx_copy(h, m * nw + j).start()
 
     def fetch(slots, runs):
         for h, m in slots:
-            for j in range(nb):
-                idx_copy(h, m * nb + j).wait()
+            for j in range(nw):
+                idx_copy(h, m * nw + j).wait()
         for h, m, n in runs:
-            first = (h * 8 + m) * cap
-
-            def gather(g, _):
-                base = pl.multiple_of(first + g * 16, 16)
-                for j in range(16):
-                    r = idx_s[base + j] & 8191
-                    picked[pl.ds(base + j, 1), :] = table[pl.ds(r, 1), :]
-                return 0
-
-            lax.fori_loop(0, n * cap // 16, gather, 0)
+            first = h * 8 + m
+
+            def list_of(k, _):
+                def gather(g, _):
+                    word = (first + k) * (nw * 128) + g * 16
+                    base = pl.multiple_of((first + k) * cap + g * 16, 16)
+                    for j in range(16):
+                        w = idx_s[word + j]
+                        picked[pl.ds(base + j, 1), :] = table[pl.ds(w & 8191, 1), :]
+                        picked[pl.ds(base + (nw * 128 + j), 1), :] = table[pl.ds(lax.shift_right_logical(w, 19), 1), :]
+                    return 0
+
+                return lax.fori_loop(0, nw * 8, gather, 0)
+
+            lax.fori_loop(0, n, list_of, 0)
         for h, m in slots:
             for j in range(nb):
                 r = m * nb + j
@@ -235,9 +241,9 @@
     g3 = [(core, m) for m in range(4, 8)]
     arrive(g0)
     arrive(g1)
+    fetch(g0, [(0, 0, 2), (1, 0, 2)])
     pl.semaphore_wait(known.at[1], 2)
     tell(known.at[2], 4)
-    fetch(g0, [(0, 0, 2), (1, 0, 2)])
     arrive(g2)
     fetch(g1, [(0, 2, 2), (1, 2, 2)])
     arrive(g3)
@@ -344,11 +350,11 @@
         scratch_shapes=[
             vmem((16, 32), BF16), vmem((64, 16), I32), vmem((64, 16), F32), vmem((32, 16384), BF16), vmem((32, 16384), BF16),
             vmem((8192, 128), F32), vmem((16, 2 * nb + 4, 128), F32), vmem((2, 8, 2 * nb + 4, 128), F32),
-            vmem((2, 8, 32, 128), BF16), vmem((2, nh, 128), I32), pltpu.SMEM((2 * nh * 128,), I32),
+            vmem((2, 8, 32, 128), BF16), vmem((2, nh // 2, 128), I32), pltpu.SMEM((nh * 128,), I32),
             vmem((2, nh, 128), I32), vmem((2, nh, 128), F32), vmem((2 * nh * 128, 128), F32),
             vmem((2, nh, 128), F32), vmem((nh, 128), F32), vmem((nh, 128), BF16), vmem((16, nh, 128), BF16),
             vmem((2, nh, 128), BF16), vmem((2, nh, 128), F32), vmem((16, 4, 128), F32), vmem((16, 4, 128), F32),
-            dma((5,)), dma((2 * nh,)), dma((16,)), dma((16,)), dma, dma, dma((16,)), dma((16,)), dma, dma,
+            dma((5,)), dma((nh,)), dma((16,)), dma((16,)), dma, dma, dma((16,)), dma((16,)), dma, dma,
             dma((16,)), dma((16,)), pltpu.SemaphoreType.REGULAR((3,)),
         ],
         compiler_params=pltpu.CompilerParams(collective_id=cid, has_side_effects=True, vmem_limit_bytes=48 << 20),

time: 43.6 us -> 42 us (0.963)
  Pallas kernels: 41.9 us -> 40.2 us
    pallas_call x1, Pallas kernels: 41.9 us -> 40.2 us  [run(): pl.pallas_call(functools.partial(kernel, cap), out_shape=(jax.ShapeDtypeS...]
where the time goes in v3:
time: 42 us; the launch traced here: 41.8 us
  Pallas kernels  40.2 us (96%)
  between operations  0.77 us (2%)
  local copies, waits for them, and re-layouts  0.61 us (1%)
    pallas_call x1, Pallas kernels, run(): pl.pallas_call(functools.partial(kernel, cap), out_shape=(jax.ShapeDtypeS...  40.2 us

profile of v3, /device:TPU:1, one launch (start us, length us, event | category | flops | bytes accessed | tf_op | source)
XLA Modules:
  0.0 41.8 jit_solution(16616242020124491741)
XLA Ops:
  0.0 0.0 copy-start.1
  0.0 0.0 copy-start.2
  0.0 0.0 copy-start.3
  0.0 0.0 copy-start.4
  0.0 0.0 copy-start.5
  0.0 40.2 %shard_map.57 = (bf16[16,32]{1,0:T(8,128)(2,1)S(1)}, s32[1,1]{1,0:T(1,128)}) custom-call(bf16[16,32]{1,0:T(8,128)(2,1)} %feat_hbm.1, bf16[32,16384]{1,0:T(8,128)(2,1)} %bitcast.58, bf16[32,16384]{1,0:T(8,128)(2,1)} %bitcast.59, s32[64,16]{1,0:T(8,128)} %bitcast.67, f32[64,16]{1,0:T(8,128)} %bitcast.70), custom_call_target="tpu_custom_call" | custom-call | tf_op jit(solution)/shard_map/pallas_call | solution.py:345
  41.0 0.0 copy-done.1
  41.0 0.0 copy-done.2
  41.0 0.0 copy-done.3
  41.0 0.0 copy-done.4
  41.0 0.0 copy-done.5
  41.0 0.2 conditional.1
  41.3 0.6 %copy.135 = bf16[16,32]{1,0:T(8,128)(2,1)} copy(bf16[16,32]{1,0:T(8,128)(2,1)S(1)} %get-tuple-element.163) | data formatting | bytes 2048
Async XLA Ops:
  0.0 41.0 %copy-start.1 = (bf16[16384,32]{0,1:T(8,128)(2,1)S(1)}, bf16[16384,32]{0,1:T(8,128)(2,1)}, u32[]{:S(2)}) copy-start(bf16[16384,32]{0,1:T(8,128)(2,1)} %param.12) | copy-start | bytes 3145732
  0.0 41.0 %copy-start.2 = (bf16[16384,32]{0,1:T(8,128)(2,1)S(1)}, bf16[16384,32]{0,1:T(8,128)(2,1)}, u32[]{:S(2)}) copy-start(bf16[16384,32]{0,1:T(8,128)(2,1)} %param.13) | copy-start | bytes 3145732
  0.0 41.0 %copy-start.3 = (s32[16,4,16]{2,1,0:T(4,128)S(1)}, s32[16,4,16]{2,1,0:T(4,128)}, u32[]{:S(2)}) copy-start(s32[16,4,16]{2,1,0:T(4,128)} %param.14) | copy-start | bytes 12292
  0.0 41.0 %copy-start.4 = (f32[16,4,16]{2,1,0:T(4,128)S(1)}, f32[16,4,16]{2,1,0:T(4,128)}, u32[]{:S(2)}) copy-start(f32[16,4,16]{2,1,0:T(4,128)} %param.15) | copy-start | bytes 12292
  0.0 41.0 %copy-start.5 = (bf16[16,32]{1,0:T(8,128)(2,1)S(1)}, bf16[16,32]{1,0:T(8,128)(2,1)}, u32[]{:S(2)}) copy-start(bf16[16,32]{1,0:T(8,128)(2,1)} %feat_hbm.1) | copy-start | bytes 3076

commit v4 on v3

--- a/solution.py
+++ b/solution.py
@@ -112,7 +112,7 @@
 def kernel(cap, feat_hbm, key_hbm, val_hbm, chosen_hbm, scores_hbm, out, flag,
            feat, chosen, scores, keys, vals, table, msg, got, fplace, idx_v, idx_s, sel_v, gate_v, picked,
            part, pair, half, zbuf, wbuf, wvec, obuf, dbuf,
-           in_sem, idx_sem, a_send, a_recv, p_send, p_recv, z_send, z_recv, w_send, w_recv, d_send, d_recv, known):
+           in_sem, idx_sem, a_send, a_recv, p_send, p_recv, z_send, z_recv, w_send, w_recv, d_send, d_recv, known, told, flag_sem):
     nb = cap // 128
     nh = 8 * nb
     nw = nb // 2
@@ -198,14 +198,14 @@
             sel_v[h, at] = lax.shift_right_logical(code, 13) & 31
             gate_v[h, at] = got[h, m, nb : 2 * nb]
         for h, m in slots:
+            for j in range(nw):
+                idx_copy(h, m * nw + j).start()
+        for h, m in slots:
             f = got[h, m, 2 * nb : 2 * nb + 4]
             f = jnp.where(keep, jnp.concatenate([f, f, f, f], axis=0), 0.0).astype(BF16)
             f = mm(f, fold).astype(BF16)
             fplace[h, m, 0:16] = f[:, 0:128]
             fplace[h, m, 16:32] = f[:, 128:256]
-        for h, m in slots:
-            for j in range(nw):
-                idx_copy(h, m * nw + j).start()
 
     def fetch(slots, runs):
         for h, m in slots:
@@ -268,7 +268,9 @@
     worst = got[0, 0, 0:nb]
     for p in range(1, 16):
         worst = jnp.maximum(worst, got[p % 2, p // 2, 0:nb])
-    flag[0, 0] = lax.shift_right_logical(jnp.max(worst).astype(I32), 18)
+    told[0, 0] = lax.shift_right_logical(jnp.max(worst).astype(I32), 18)
+    flag_copy = pltpu.make_async_copy(told, flag, flag_sem)
+    flag_copy.start()
     for d in RING:
         z_copy(d).wait_recv()
     whole = zbuf[0].astype(F32)
@@ -335,6 +337,7 @@
         out_copy(p % 2, p // 2).wait_send()
     pair_copy.wait_send()
     w_copy.wait_send()
+    flag_copy.wait()
 
 
 def run(cap, cid, feat, key_t, val_t, chosen, scores):
@@ -346,7 +349,7 @@
         functools.partial(kernel, cap),
         out_shape=(jax.ShapeDtypeStruct((16, 32), BF16), jax.ShapeDtypeStruct((1, 1), I32)),
         in_specs=[pl.BlockSpec(memory_space=pl.ANY)] * 5,
-        out_specs=(pl.BlockSpec(memory_space=vmem), pl.BlockSpec(memory_space=pltpu.SMEM)),
+        out_specs=(pl.BlockSpec(memory_space=vmem), pl.BlockSpec(memory_space=pl.ANY)),
         scratch_shapes=[
             vmem((16, 32), BF16), vmem((64, 16), I32), vmem((64, 16), F32), vmem((32, 16384), BF16), vmem((32, 16384), BF16),
             vmem((8192, 128), F32), vmem((16, 2 * nb + 4, 128), F32), vmem((2, 8, 2 * nb + 4, 128), F32),
@@ -355,7 +358,7 @@
             vmem((2, nh, 128), F32), vmem((nh, 128), F32), vmem((nh, 128), BF16), vmem((16, nh, 128), BF16),
             vmem((2, nh, 128), BF16), vmem((2, nh, 128), F32), vmem((16, 4, 128), F32), vmem((16, 4, 128), F32),
             dma((5,)), dma((nh,)), dma((16,)), dma((16,)), dma, dma, dma((16,)), dma((16,)), dma, dma,
-            dma((16,)), dma((16,)), pltpu.SemaphoreType.REGULAR((3,)),
+            dma((16,)), dma((16,)), pltpu.SemaphoreType.REGULAR((3,)), pltpu.SMEM((1, 1), I32), dma,
         ],
         compiler_params=pltpu.CompilerParams(collective_id=cid, has_side_effects=True, vmem_limit_bytes=48 << 20),
     )(feat, key_t, val_t, chosen, scores)

time: 42 us -> 41.5 us (0.988)
  Pallas kernels: 40.2 us -> 39.7 us
    pallas_call x1, Pallas kernels: 40.2 us -> 39.7 us  [run(): pl.pallas_call(functools.partial(kernel, cap), out_shape=(jax.ShapeDtypeS...]
where the time goes in v4:
time: 41.5 us; the launch traced here: 41.4 us
  Pallas kernels  39.7 us (96%)
  between operations  0.77 us (2%)
  local copies, waits for them, and re-layouts  0.61 us (1%)
    pallas_call x1, Pallas kernels, run(): pl.pallas_call(functools.partial(kernel, cap), out_shape=(jax.ShapeDtypeS...  39.7 us

profile of v4, /device:TPU:1, one launch (start us, length us, event | category | flops | bytes accessed | tf_op | source)
XLA Modules:
  0.0 41.4 jit_solution(10361499405190596165)
XLA Ops:
  0.0 0.0 copy-start.1
  0.0 0.0 copy-start.2
  0.0 0.0 copy-start.3
  0.0 0.0 copy-start.4
  0.0 0.0 copy-start.5
  0.0 39.7 %shard_map.57 = (bf16[16,32]{1,0:T(8,128)(2,1)S(1)}, s32[1,1]{1,0:T(1,128)}) custom-call(bf16[16,32]{1,0:T(8,128)(2,1)} %feat_hbm.1, bf16[32,16384]{1,0:T(8,128)(2,1)} %bitcast.58, bf16[32,16384]{1,0:T(8,128)(2,1)} %bitcast.59, s32[64,16]{1,0:T(8,128)} %bitcast.67, f32[64,16]{1,0:T(8,128)} %bitcast.70), custom_call_target="tpu_custom_call" | custom-call | tf_op jit(solution)/shard_map/pallas_call | solution.py:348
  40.5 0.0 copy-done.1
  40.5 0.0 copy-done.2
  40.5 0.0 copy-done.3
  40.5 0.0 copy-done.4
  40.5 0.0 copy-done.5
  40.5 0.2 conditional.1
  40.8 0.6 %copy.135 = bf16[16,32]{1,0:T(8,128)(2,1)} copy(bf16[16,32]{1,0:T(8,128)(2,1)S(1)} %get-tuple-element.163) | data formatting | bytes 2048
Async XLA Ops:
  0.0 40.5 %copy-start.1 = (bf16[16384,32]{0,1:T(8,128)(2,1)S(1)}, bf16[16384,32]{0,1:T(8,128)(2,1)}, u32[]{:S(2)}) copy-start(bf16[16384,32]{0,1:T(8,128)(2,1)} %param.12) | copy-start | bytes 3145732
  0.0 40.5 %copy-start.2 = (bf16[16384,32]{0,1:T(8,128)(2,1)S(1)}, bf16[16384,32]{0,1:T(8,128)(2,1)}, u32[]{:S(2)}) copy-start(bf16[16384,32]{0,1:T(8,128)(2,1)} %param.13) | copy-start | bytes 3145732
  0.0 40.5 %copy-start.3 = (s32[16,4,16]{2,1,0:T(4,128)S(1)}, s32[16,4,16]{2,1,0:T(4,128)}, u32[]{:S(2)}) copy-start(s32[16,4,16]{2,1,0:T(4,128)} %param.14) | copy-start | bytes 12292
  0.0 40.5 %copy-start.4 = (f32[16,4,16]{2,1,0:T(4,128)S(1)}, f32[16,4,16]{2,1,0:T(4,128)}, u32[]{:S(2)}) copy-start(f32[16,4,16]{2,1,0:T(4,128)} %param.15) | copy-start | bytes 12292
  0.0 40.5 %copy-start.5 = (bf16[16,32]{1,0:T(8,128)(2,1)S(1)}, bf16[16,32]{1,0:T(8,128)(2,1)}, u32[]{:S(2)}) copy-start(bf16[16,32]{1,0:T(8,128)(2,1)} %feat_hbm.1) | copy-start | bytes 3076
